TPU v7x, 32 devices: a whole 2x2x4 slice. The times are simulated.
32 devices in a mesh: sp: 8 (over z, y), tp: 4 (over x, core).
Axes of the slice: x: 2, y: 2, z: 4, core: 2. Of those that a mesh axis runs over, the one named last changes fastest.
Arguments:
- resid_in: bfloat16 [3072, 2048], P('sp'), may hold values from -6 to 6
- cotangent: bfloat16 [3072, 2048], P('sp'), may hold values from -2 to 2
- norm_gain: float32 [2048], replicated, may hold values from 0.1 to 1.9
- routes: int32 [3072, 2], P('sp'), may hold values from 0 to 7, all different within a row; in each aligned block of 384 rows (0 to 383, 384 to 767, ...) at most 192 rows name the same one
- route_weights: float32 [3072, 2], P('sp'), may hold values from 0.1 to 1
- gate_weight: bfloat16 [8, 2048, 1024], P('sp', None, 'tp'), may hold values from -0.125 to 0.125
- up_weight: bfloat16 [8, 2048, 1024], P('sp', None, 'tp'), may hold values from -0.125 to 0.125
- down_weight: bfloat16 [8, 1024, 2048], P('sp', 'tp'), may hold values from -0.1875 to 0.1875
- out_weight: bfloat16 [2048, 1024], P(None, 'tp'), may hold values from -0.1875 to 0.1875
- gate_b: bfloat16 [3072, 1024], P('sp', 'tp'), may hold values from -6 to 6
- gate_c: bfloat16 [3072, 1024], P('sp', 'tp'), may hold values from -6 to 6
- values_u: bfloat16 [3072, 1024], P('sp', 'tp'), may hold values from -6 to 6
- taps: float32 [3, 1024], P(None, 'tp'), may hold values from -3.5 to 3.5
Outputs:
- grad_gate_weight: float32 [8, 2048, 1024], P('sp', None, 'tp')
- grad_up_weight: float32 [8, 2048, 1024], P('sp', None, 'tp')
- grad_down_weight: float32 [8, 1024, 2048], P('sp', 'tp')
- grad_resid: bfloat16 [3072, 2048], P('sp')
- grad_out_weight: float32 [2048, 1024], P('sp', 'tp')
- grad_gate_b: bfloat16 [3072, 1024], P('sp', 'tp')
- grad_gate_c: bfloat16 [3072, 1024], P('sp', 'tp')
- grad_values: bfloat16 [3072, 1024], P('sp', 'tp')
Inputs may be any that keep to these rules, and one draw needn't show every extreme that they name: `routes`: A row's 2 experts differ. In the rows of one index of sp (384 tokens) no expert is named more than 192 times, a bound that some block reaches.
All inputs are finite; a program needn't handle non-finite values.
Results may differ from a plain program's by a relative error of at most 0.024.
Values may be sent and summed in bfloat16 or wider, within the bound.
A program may use at most 128 MiB of HBM per device.

v0:
```python
import jax
import jax.numpy as jnp
from jax import lax
from jax.sharding import PartitionSpec as P

norm_eps = 1e-06


def passed_along(array, axis, by):
    size = lax.axis_size(axis)
    pairs = [(i, i + by) for i in range(size) if 0 <= i + by < size]
    return lax.ppermute(array, axis, pairs)


def expert_pass(entry_rows, entry_cots, entry_weights, gate_mat, up_mat, down_mat):
    f32 = jnp.float32
    bf16 = jnp.bfloat16
    gate_pre = jnp.dot(entry_rows, gate_mat, preferred_element_type=f32)
    up_pre = jnp.dot(entry_rows, up_mat, preferred_element_type=f32)
    logistic = jax.nn.sigmoid(gate_pre)
    activated = gate_pre * logistic
    hidden = (activated * up_pre * entry_weights[:, None]).astype(bf16)
    grad_down = jnp.einsum("rf,rd->fd", hidden, entry_cots, preferred_element_type=f32)
    dhidden = (
        jnp.einsum("rd,fd->rf", entry_cots, down_mat, preferred_element_type=f32)
        * entry_weights[:, None]
    )
    dgate = (dhidden * up_pre * logistic * (1.0 + gate_pre * (1.0 - logistic))).astype(bf16)
    dup = (dhidden * activated).astype(bf16)
    grad_gate = jnp.einsum("rd,rf->df", entry_rows, dgate, preferred_element_type=f32)
    grad_up = jnp.einsum("rd,rf->df", entry_rows, dup, preferred_element_type=f32)
    partial_sum = jnp.einsum("rf,df->rd", dgate, gate_mat, preferred_element_type=f32) + jnp.einsum(
        "rf,df->rd", dup, up_mat, preferred_element_type=f32
    )
    return (grad_gate, grad_up, grad_down, partial_sum)


def on_device(
    resid_in,
    cotangent,
    norm_gain,
    routes,
    route_weights,
    gate_weight,
    up_weight,
    down_weight,
    out_weight,
    gate_b,
    gate_c,
    values_u,
    taps,
):
    f32 = jnp.float32
    bf16 = jnp.bfloat16
    token_count, model_width = resid_in.shape
    groups = lax.axis_size("sp")
    lanes = lax.axis_size("tp")
    local_experts = gate_weight.shape[0]
    expert_total = local_experts * groups
    capacity = 4 * token_count // expert_total
    slot_span = local_experts * capacity
    resid_wide = resid_in.astype(f32)
    inv_rms = lax.rsqrt(jnp.mean(resid_wide * resid_wide, axis=1, keepdims=True) + norm_eps)
    normed = (resid_wide * inv_rms * norm_gain).astype(bf16)
    mixed = gate_c.astype(f32) * values_u.astype(f32)
    earlier = passed_along(mixed[-2:], "sp", 1)
    quarter = model_width // lanes
    lane = lax.axis_index("tp")
    slots = expert_total * capacity
    names = jnp.arange(expert_total, dtype=jnp.int32)
    chosen = routes[:, :, None] == names[None, None, :]
    named = jnp.any(chosen, axis=1).astype(bf16)
    order = jnp.arange(token_count, dtype=jnp.int32)
    strict = (order[:, None] > order[None, :]).astype(bf16)
    before = jnp.dot(strict, named, preferred_element_type=f32).astype(jnp.int32)
    rank = jnp.sum(jnp.where(chosen, before[:, None, :], 0), axis=2)
    targets = routes * capacity + rank
    slot_ids = jnp.arange(slots, dtype=jnp.int32)[:, None]
    first = slot_ids == targets[:, 0][None, :]
    second = slot_ids == targets[:, 1][None, :]
    placing = (first | second).astype(bf16)
    sent_weights = jnp.sum(
        jnp.where(first, route_weights[:, 0][None, :], 0.0)
        + jnp.where(second, route_weights[:, 1][None, :], 0.0),
        axis=1,
    ).reshape(groups, slot_span)
    own_rows = lax.dynamic_slice_in_dim(normed, lane * quarter, quarter, axis=1)
    own_cots = lax.dynamic_slice_in_dim(cotangent, lane * quarter, quarter, axis=1)
    sent_rows = jnp.dot(placing, own_rows, preferred_element_type=f32).astype(bf16)
    sent_cots = jnp.dot(placing, own_cots, preferred_element_type=f32).astype(bf16)
    sent_rows = sent_rows.reshape(groups, slot_span, quarter)
    sent_cots = sent_cots.reshape(groups, slot_span, quarter)
    got_weights = lax.all_to_all(sent_weights, "sp", split_axis=0, concat_axis=0, tiled=True)
    got_rows = lax.all_gather(
        lax.all_to_all(sent_rows, "sp", split_axis=0, concat_axis=0, tiled=True),
        "tp",
        axis=2,
        tiled=True,
    )
    got_cots = lax.all_gather(
        lax.all_to_all(sent_cots, "sp", split_axis=0, concat_axis=0, tiled=True),
        "tp",
        axis=2,
        tiled=True,
    )
    grads_gate, grads_up, grads_down, terms = ([], [], [], [])
    entry_rows = got_rows.reshape(groups * capacity, model_width)
    entry_cots = got_cots.reshape(groups * capacity, model_width)
    entry_weights = got_weights.reshape(groups * capacity)
    grad_gate, grad_up, grad_down, partial_sum = expert_pass(
        entry_rows, entry_cots, entry_weights, gate_weight[0], up_weight[0], down_weight[0]
    )
    grads_gate.append(grad_gate)
    grads_up.append(grad_up)
    grads_down.append(grad_down)
    terms.append(partial_sum.astype(bf16).reshape(groups, capacity, model_width))
    expert_term = terms[0]
    summed = (
        lax.psum_scatter(expert_term, "tp", scatter_dimension=2, tiled=True)
        .astype(jnp.float32)
        .astype(bf16)
    )
    returned = lax.all_to_all(summed, "sp", split_axis=0, concat_axis=0, tiled=True).reshape(
        expert_total * capacity, model_width // lanes
    )
    own_grad = jnp.einsum("st,sq->tq", placing, returned, preferred_element_type=f32)
    dnormed = lax.all_gather(own_grad.astype(bf16), "tp", axis=1, tiled=True).astype(f32)
    scaled = dnormed * norm_gain
    resid_grad = (
        cotangent.astype(f32)
        + inv_rms * scaled
        - resid_wide * inv_rms**3 * jnp.mean(scaled * resid_wide, axis=1, keepdims=True)
    )
    grad_resid = resid_grad.astype(bf16)
    extended = jnp.concatenate([earlier, mixed], axis=0)
    conv = (
        taps[0] * extended[:token_count]
        + taps[1] * extended[1 : token_count + 1]
        + taps[2] * extended[2 : token_count + 2]
    )
    merged = (gate_b.astype(f32) * conv).astype(bf16)
    grad_out_weight = lax.psum_scatter(
        jnp.einsum("td,tc->dc", grad_resid, merged, preferred_element_type=f32).astype(
            jnp.bfloat16
        ),
        "sp",
        scatter_dimension=0,
        tiled=True,
    ).astype(jnp.float32)
    dmerged = jnp.dot(grad_resid, out_weight, preferred_element_type=f32)
    grad_gate_b = (dmerged * conv).astype(bf16)
    dconv = dmerged * gate_b.astype(f32)
    later = passed_along(dconv[:2], "sp", -1)
    extended_grad = jnp.concatenate([dconv, later], axis=0)
    dmixed = (
        taps[2] * extended_grad[:token_count]
        + taps[1] * extended_grad[1 : token_count + 1]
        + taps[0] * extended_grad[2 : token_count + 2]
    )
    grad_gate_c = (dmixed * values_u.astype(f32)).astype(bf16)
    grad_values = (dmixed * gate_c.astype(f32)).astype(bf16)
    return (
        jnp.stack(grads_gate),
        jnp.stack(grads_up),
        jnp.stack(grads_down),
        grad_resid,
        grad_out_weight,
        grad_gate_b,
        grad_gate_c,
        grad_values,
    )


def solution(mesh):
    placed = (
        P("sp", None),
        P("sp", None),
        P(),
        P("sp", None),
        P("sp", None),
        P("sp", None, "tp"),
        P("sp", None, "tp"),
        P("sp", "tp", None),
        P(None, "tp"),
        P("sp", "tp"),
        P("sp", "tp"),
        P("sp", "tp"),
        P(None, "tp"),
    )
    return jax.shard_map(
        on_device,
        mesh=mesh,
        in_specs=placed,
        out_specs=(
            P("sp", None, "tp"),
            P("sp", None, "tp"),
            P("sp", "tp", None),
            P("sp", None),
            P("sp", "tp"),
            P("sp", "tp"),
            P("sp", "tp"),
            P("sp", "tp"),
        ),
        check_vma=False,
    )
```

profile of v0, /device:TPU:0, one launch (start us, length us, event | category | flops | bytes accessed | tf_op | source)
XLA Modules:
  0.0 364.5 jit_solution(5835447940842580865)
XLA Ops:
  7.2 0.0 copy-start
  7.2 0.0 all-gather.4.cloned.1.call-start
  7.3 3.6 convert_element_type.75
  10.8 0.4 multiply_reduce_fusion.1
  11.2 0.0 copy-done.14
  11.2 0.1 convolution_convert_fusion.3
  11.4 0.1 select_reduce_fusion
  11.5 0.1 dynamic-slice
  11.6 2.2 convolution_convert_fusion.1
  13.8 44.2 %all_to_all.24 = bf16[8,192,512]{2,1,0:T(8,128)(2,1)} all-to-all(bf16[8,192,512]{2,1,0:T(8,128)(2,1)S(1)} %bitcast.47), channel_id=1, replica_groups=mesh['sp'=8,'tp'=4] {'sp'}, dimensions={0} | all-to-all | bytes 3145728 | tf_op jit(solution)/shard_map/all_to_all | solution.py:95
  58.0 0.0 all-gather.4.cloned.1.call-update
  58.0 0.0 all-gather.6.cloned.1.call-start
  58.1 2.0 convolution_convert_fusion
  60.1 0.0 copy-start.15
  60.1 40.2 %all_to_all.25 = bf16[8,192,512]{2,1,0:T(8,128)(2,1)} all-to-all(bf16[8,192,512]{2,1,0:T(8,128)(2,1)S(1)} %bitcast.48), channel_id=1, replica_groups=mesh['sp'=8,'tp'=4] {'sp'}, dimensions={0} | all-to-all | bytes 3145728 | tf_op jit(solution)/shard_map/all_to_all | solution.py:101
  100.3 0.0 all-gather.6.cloned.1.call-update
  100.3 0.0 reduce-scatter.3.cloned.1.call-start
  100.4 0.6 add_reduce_fusion
  101.0 0.1 all_to_all.17
  101.0 9.9 %all_to_all.26 = f32[8,1,192]{2,1,0:T(1,128)S(1)} all-to-all(f32[8,1,192]{2,1,0:T(1,128)S(1)} %all_to_all.17), channel_id=1, replica_groups=mesh['sp'=8,'tp'=4] {'sp'}, dimensions={0} | all-to-all | bytes 12288 | tf_op jit(solution)/shard_map/all_to_all | solution.py:93
  110.9 0.1 mul.171
  111.0 6.7 %fusion.17 = f32[1536,256]{1,0:T(8,128)} fusion(bf16[1536,2048]{1,0:T(8,128)(2,1)} %bitcast.55, bf16[1,2048,256]{2,1,0:T(8,128)(2,1)S(1)} %copy-done), kind=kOutput, calls=%fused_computation.32 | convolution fusion | flops 1610612736 | bytes 8912896 | tf_op jit(solution)/shard_map/dot_general | solution.py:18
  117.7 0.0 copy-done.5
  117.7 0.5 copy-done.17
  118.2 3.0 fusion.20
  121.2 30.3 %all-gather.6.cloned.1.call-done = bf16[8,192,2048]{2,1,0:T(8,128)(2,1)} async-done(((bf16[8,192,512]{2,1,0:T(8,128)(2,1)}), bf16[8,192,2048]{2,1,0:T(8,128)(2,1)}) %all-gather.6.cloned.1.call-update) | async-done | bytes 6291472 | tf_op jit(solution)/shard_map/all_gather | solution.py:100
  151.5 6.4 %multiply_convert_fusion.1 = (bf16[1536,256]{1,0:T(8,128)(2,1)S(1)}, bf16[1536,256]{1,0:T(8,128)(2,1)S(1)}) fusion(f32[1536,256]{1,0:T(8,128)} %fusion.17, f32[1536,256]{1,0:T(8,128)} %fusion.20, f32[1536]{0:T(1024)S(1)} %mul.171, bf16[1536,2048]{1,0:T(8,128)(2,1)} %bitcast.59, bf16[1,256,2048]{2,1,0:T(8,128)(2,1)} %param.20), kind=kOutput, calls=%fused_computation.17 | convolution fusion | flops 1616117760 | bytes 12064768 | tf_op jit(solution)/shard_map/rd,fd->rf/dot_general | solution.py:25
  158.0 0.0 copy-start.7
  158.0 0.0 copy-start.6
  158.0 1.8 fusion.15
  159.8 0.0 copy-done.7
  159.8 0.0 copy-done.6
  159.8 4.4 %add_convert_fusion = bf16[1536,2048]{1,0:T(8,128)(2,1)} fusion(f32[1536,2048]{1,0:T(8,128)S(1)} %fusion.15, bf16[1536,256]{1,0:T(8,128)(2,1)S(1)} %get-tuple-element.16, bf16[1,2048,256]{2,1,0:T(8,128)(2,1)S(1)} %copy-done.6), kind=kOutput, calls=%fused_computation | convolution fusion | flops 1616904192 | bytes 20709376 | tf_op jit(solution)/shard_map/rf,df->rd/dot_general | solution.py:32
  164.3 0.0 reduce-scatter.3.cloned.1.call-update
  164.3 0.0 all-gather.8.cloned.1.call-start
  164.3 58.0 %reduce-scatter.3.cloned.1.call-done = bf16[8,192,512]{2,1,0:T(8,128)(2,1)} async-done(((bf16[8,192,2048]{2,1,0:T(8,128)(2,1)}), bf16[8,192,512]{2,1,0:T(8,128)(2,1)}) %reduce-scatter.3.cloned.1.call-update) | async-done | bytes 1572880 | tf_op jit(solution)/shard_map/reduce_scatter | solution.py:119
  222.3 42.4 %all_to_all.27 = bf16[8,192,512]{2,1,0:T(8,128)(2,1)S(1)} all-to-all(bf16[8,192,512]{2,1,0:T(8,128)(2,1)} %reduce-scatter.3.cloned.1.call-done), channel_id=1, replica_groups=mesh['sp'=8,'tp'=4] {'sp'}, dimensions={0} | all-to-all | bytes 3145728 | tf_op jit(solution)/shard_map/all_to_all | solution.py:123
  264.7 1.6 fusion.6
  266.3 0.0 all-gather.8.cloned.1.call-update
  266.3 0.0 reduce-scatter.5.cloned.1.call-start
  266.3 0.0 copy-done.9
  266.4 3.6 collective-permute-start
  270.0 14.1 %all-gather.8.cloned.1.call-done = bf16[384,2048]{1,0:T(8,128)(2,1)} async-done(((bf16[384,512]{1,0:T(8,128)(2,1)}), bf16[384,2048]{1,0:T(8,128)(2,1)}) %all-gather.8.cloned.1.call-update) | async-done | bytes 1572880 | tf_op jit(solution)/shard_map/all_gather | solution.py:127
  284.1 2.1 multiply_reduce_fusion
  286.3 0.0 copy-start.18
  286.3 0.0 copy-start.19
  286.3 2.5 subtract_convert_fusion
  288.8 0.0 copy-start.4
  288.8 0.0 collective-permute-done
  288.9 1.3 multiply_convert_fusion.4
  290.2 1.8 convolution_convert_fusion.2
  292.0 0.0 reduce-scatter.5.cloned.1.call-update
  292.0 0.0 copy-start.20
  292.0 0.0 copy-start.21
  292.0 6.2 %convolution_bitcast_fusion.2 = f32[1,2048,256]{2,1,0:T(8,128)} fusion(bf16[1536,2048]{1,0:T(8,128)(2,1)} %bitcast.56, bf16[1536,256]{1,0:T(8,128)(2,1)S(1)} %get-tuple-element.17), kind=kOutput, calls=%fused_computation.10 | convolution fusion | flops 1610612736 | bytes 9175040 | tf_op jit(solution)/shard_map/rd,rf->df/dot_general | solution.py:30
  298.2 6.3 %convolution_bitcast_fusion = f32[1,256,2048]{2,1,0:T(8,128)} fusion(bf16[1536,2048]{1,0:T(8,128)(2,1)} %bitcast.60, f32[1536,256]{1,0:T(8,128)S(1)} %copy-done.21, f32[1536]{0:T(1024)S(1)} %mul.171, f32[1536,256]{1,0:T(8,128)S(1)} %copy-done.20), kind=kOutput, calls=%fused_computation.8 | convolution fusion | flops 1613365248 | bytes 11540480 | tf_op jit(solution)/shard_map/rf,rd->fd/dot_general | solution.py:23
  304.5 1.4 collective-permute-start.1
  305.9 0.0 copy-start.1
  305.9 6.1 %convolution_bitcast_fusion.1 = f32[1,2048,256]{2,1,0:T(8,128)} fusion(bf16[1536,2048]{1,0:T(8,128)(2,1)} %bitcast.57, bf16[1536,256]{1,0:T(8,128)(2,1)S(1)} %copy-done.8), kind=kOutput, calls=%fused_computation.9 | convolution fusion | flops 1610612736 | bytes 9175040 | tf_op jit(solution)/shard_map/rd,rf->df/dot_general | solution.py:31
  312.0 0.0 collective-permute-done.1
  312.0 0.8 fusion.35
  312.9 0.7 fusion.36
  313.6 42.8 %reduce-scatter.5.cloned.1.call-done = bf16[256,256]{1,0:T(8,128)(2,1)} async-done(((bf16[2048,256]{1,0:T(8,128)(2,1)}), bf16[256,256]{1,0:T(8,128)(2,1)}) %reduce-scatter.5.cloned.1.call-update) | async-done | bytes 131088 | tf_op jit(solution)/shard_map/reduce_scatter | solution.py:142
  356.3 1.6 convert_element_type.92
  (40 shorter events, 0.2 us)
Async XLA Ops:
  7.2 103.8 %copy-start = (bf16[1,2048,256]{2,1,0:T(8,128)(2,1)S(1)}, bf16[1,2048,256]{2,1,0:T(8,128)(2,1)}, u32[]{:S(2)}) copy-start(bf16[1,2048,256]{2,1,0:T(8,128)(2,1)} %param.18) | copy-start | bytes 3145732
  7.2 103.8 %all-gather.4.cloned.1.call-start = ((), (), s32[]{:S(2)}) async-start(), calls=%async_computation.6 | async-start | bytes 7864320 | tf_op jit(solution)/shard_map/all_gather | solution.py:94
  7.2 3.6 copy-start.2
  7.2 4.0 %copy-start.14 = (s32[384,2]{0,1:T(2,128)S(1)}, s32[384,2]{0,1:T(2,128)}, u32[]{:S(2)}) copy-start(s32[384,2]{0,1:T(2,128)} %param.16) | copy-start | bytes 9220
  7.3 4.3 %copy-start.13 = (f32[2048]{0:T(1024)S(1)}, f32[2048]{0:T(1024)}, u32[]{:S(2)}) copy-start(f32[2048]{0:T(1024)} %param.15) | copy-start | bytes 24580
  58.0 93.5 %all-gather.6.cloned.1.call-start = ((), (), s32[]{:S(2)}) async-start(), calls=%async_computation.7 | async-start | bytes 7864320 | tf_op jit(solution)/shard_map/all_gather | solution.py:100
  60.1 40.3 %copy-start.15 = (f32[384,2]{0,1:T(2,128)S(1)}, f32[384,2]{0,1:T(2,128)}, u32[]{:S(2)}) copy-start(f32[384,2]{0,1:T(2,128)} %param.17) | copy-start | bytes 9220
  100.3 122.0 %reduce-scatter.3.cloned.1.call-start = ((), (), s32[]{:S(2)}) async-start(), calls=%async_computation.8 | async-start | bytes 7864320 | tf_op jit(solution)/shard_map/reduce_scatter | solution.py:119
  111.0 6.7 %copy-start.5 = (bf16[1,2048,256]{2,1,0:T(8,128)(2,1)S(1)}, bf16[1,2048,256]{2,1,0:T(8,128)(2,1)}, u32[]{:S(2)}) copy-start(bf16[1,2048,256]{2,1,0:T(8,128)(2,1)} %param.19) | copy-start | bytes 3145732
  111.0 7.2 %copy-start.17 = (bf16[8,192,2048]{2,1,0:T(8,128)(2,1)S(1)}, bf16[8,192,2048]{2,1,0:T(8,128)(2,1)}, u32[]{:S(2)}) copy-start(bf16[8,192,2048]{2,1,0:T(8,128)(2,1)} %all-gather.4.cloned.1.call-done) | copy-start | bytes 18874372
  158.0 1.9 copy-start.7
  158.0 1.9 copy-start.6
  164.3 119.9 %all-gather.8.cloned.1.call-start = ((), (), s32[]{:S(2)}) async-start(), calls=%async_computation.9 | async-start | bytes 1966080 | tf_op jit(solution)/shard_map/all_gather | solution.py:127
  264.7 1.7 copy-start.9
  264.7 1.7 copy-start.11
  264.7 5.3 %copy-start.16 = (f32[3,256]{1,0:T(4,128)S(1)}, f32[3,256]{1,0:T(4,128)}, u32[]{:S(2)}) copy-start(f32[3,256]{1,0:T(4,128)} %param.25) | copy-start | bytes 9220
  266.3 90.0 %reduce-scatter.5.cloned.1.call-start = ((), (), s32[]{:S(2)}) async-start(), calls=%async_computation.10 | async-start | bytes 1179648 | tf_op jit(solution)/shard_map/reduce_scatter | solution.py:142
  266.4 22.4 %collective-permute-start = (f32[2,256]{1,0:T(2,128)S(1)}, f32[2,256]{1,0:T(2,128)S(1)}, u32[]{:S(2)}, u32[]{:S(2)}) collective-permute-start(f32[2,256]{1,0:T(2,128)S(1)} %slice.57), channel_id=1, source_target_pairs={{0,4},{4,8},{8,12},{12,16},{16,20},{20,24},{24,28},{1,5},{5,9},{9,... | collective-permute-start | bytes 6152 | tf_op jit(solution)/shard_map/ppermute | solution.py:12
  284.1 2.1 copy-start.3
  286.3 2.6 copy-start.18
  286.3 2.6 copy-start.19
  288.8 1.3 copy-start.4
  292.0 6.2 %copy-start.20 = (f32[1536,256]{1,0:T(8,128)S(1)}, f32[1536,256]{1,0:T(8,128)}, u32[]{:S(2)}) copy-start(f32[1536,256]{1,0:T(8,128)} %fusion.17) | copy-start | bytes 4718596
  292.0 6.2 %copy-start.21 = (f32[1536,256]{1,0:T(8,128)S(1)}, f32[1536,256]{1,0:T(8,128)}, u32[]{:S(2)}) copy-start(f32[1536,256]{1,0:T(8,128)} %fusion.20) | copy-start | bytes 4718596
  298.2 7.7 %copy-start.8 = (bf16[1536,256]{1,0:T(8,128)(2,1)S(1)}, bf16[1536,256]{1,0:T(8,128)(2,1)}, u32[]{:S(2)}) copy-start(bf16[1536,256]{1,0:T(8,128)(2,1)} %copy-done.7) | copy-start | bytes 2359300
  304.5 7.6 %copy-start.12 = (bf16[384,256]{1,0:T(8,128)(2,1)S(1)}, bf16[384,256]{1,0:T(8,128)(2,1)}, u32[]{:S(2)}) copy-start(bf16[384,256]{1,0:T(8,128)(2,1)} %param.23) | copy-start | bytes 589828
  304.5 8.4 %copy-start.10 = (bf16[384,256]{1,0:T(8,128)(2,1)S(1)}, bf16[384,256]{1,0:T(8,128)(2,1)}, u32[]{:S(2)}) copy-start(bf16[384,256]{1,0:T(8,128)(2,1)} %param.24) | copy-start | bytes 589828
  304.5 7.6 %collective-permute-start.1 = (f32[2,256]{1,0:T(2,128)S(1)}, f32[2,256]{1,0:T(2,128)S(1)}, u32[]{:S(2)}, u32[]{:S(2)}) collective-permute-start(f32[2,256]{1,0:T(2,128)S(1)} %slice.60), channel_id=1, source_target_pairs={{4,0},{8,4},{12,8},{16,12},{20,16},{24,20},{28,24},{5,1},{9,5},{13... | collective-permute-start | bytes 6152 | tf_op jit(solution)/shard_map/ppermute | solution.py:12
  305.9 52.1 %copy-start.1 = (bf16[1,2048,256]{2,1,0:T(8,128)(2,1)S(1)}, bf16[1,2048,256]{2,1,0:T(8,128)(2,1)}, u32[]{:S(2)}) copy-start(bf16[1,2048,256]{2,1,0:T(8,128)(2,1)} %param.18) | copy-start | bytes 3145732
Sparse Core Ops, SparseCore 0:
  58.2 45.3 all-gather.3
  105.1 46.3 all-gather.5
  164.4 57.8 reduce-scatter.2
  266.4 17.6 all-gather.7
  292.1 64.1 reduce-scatter.4
where the time goes:
time: 365 us; the launch traced here: 364 us
  waiting for transfers between devices  145 us (40%)
  blocking collectives  137 us (38%)
  matrix products  49.9 us (14%)
  between operations  14.1 us (4%)
  other arithmetic  12.5 us (3%)
  starting transfers between devices  5.21 us (1%)
    reduce_scatter x1, waiting for transfers between devices, on_device(): lax.psum_scatter(expert_term, 'tp', scatter_dimension=2, tiled=True)  58 us
    all_to_all x1, blocking collectives, on_device(): lax.all_to_all(sent_rows, 'sp', split_axis=0, concat_axis=0, tiled=True)  44.2 us
    reduce_scatter x1, waiting for transfers between devices, on_device(): lax.psum_scatter(jnp.einsum('td,tc->dc', grad_resid, merged, preferred_el...  42.8 us
    all_to_all x1, blocking collectives, on_device(): lax.all_to_all(summed, 'sp', split_axis=0, concat_axis=0, tiled=True)  42.4 us
    all_to_all x1, blocking collectives, on_device(): lax.all_to_all(sent_cots, 'sp', split_axis=0, concat_axis=0, tiled=True)  40.2 us
    all_gather x1, waiting for transfers between devices, on_device(): lax.all_gather(lax.all_to_all(sent_cots, 'sp', split_axis=0, concat_axis=...  30.3 us
    all_gather x1, waiting for transfers between devices, on_device(): lax.all_gather(own_grad.astype(bf16), 'tp', axis=1, tiled=True).astype(f32)  14.1 us
    all_to_all x1, blocking collectives, on_device(): lax.all_to_all(sent_weights, 'sp', split_axis=0, concat_axis=0, tiled=True)  9.85 us
  transfers between devices with their start and end apart: 7, of which 4 were waited for; matrix products, arithmetic and copies ran while one was open for 10% of the time, Pallas kernels for 0%

commit v1 on v0

--- a/solution.py
+++ b/solution.py
@@ -97,11 +97,11 @@
         axis=2,
         tiled=True,
     )
-    got_cots = lax.all_gather(
-        lax.all_to_all(sent_cots, "sp", split_axis=0, concat_axis=0, tiled=True),
-        "tp",
+    got_cots = jnp.concatenate(
+        lax.all_gather(
+            lax.all_to_all(sent_cots, "sp", split_axis=0, concat_axis=0, tiled=True), "tp"
+        ),
         axis=2,
-        tiled=True,
     )
     grads_gate, grads_up, grads_down, terms = ([], [], [], [])
     entry_rows = got_rows.reshape(groups * capacity, model_width)

time: 365 us -> 377 us (1.033)
  local copies, waits for them, and re-layouts: 0.9 us -> 16.8 us
  matrix products: 49.9 us -> 43.4 us
    reshape x0 -> x1, local copies, waits for them, and re-layouts: none -> 10.2 us  [on_device(): jnp.concatenate(lax.all_gather(lax.all_to_all(sent_cots, 'sp', split_axis...]
    unnamed x44 -> x63, local copies, waits for them, and re-layouts: 0.61 us -> 6.3 us
  transfers between devices with their start and end apart: 7 -> 7, of which waited for: 4 -> 4; matrix products, arithmetic and copies ran while one was open for 10% -> 9% of each run, Pallas kernels for 0% -> 0%
where the time goes in v1:
time: 377 us
  waiting for transfers between devices  148 us (39%)
  blocking collectives  137 us (36%)
  matrix products  43.4 us (12%)
  local copies, waits for them, and re-layouts  16.8 us (4%)
  between operations  14.2 us (4%)
  other arithmetic  12.5 us (3%)
  starting transfers between devices  5.25 us (1%)
    reduce_scatter x1, waiting for transfers between devices, on_device(): lax.psum_scatter(expert_term, 'tp', scatter_dimension=2, tiled=True)  58 us
    reduce_scatter x1, waiting for transfers between devices, on_device(): lax.psum_scatter(jnp.einsum('td,tc->dc', grad_resid, merged, preferred_el...  45.7 us
    all_to_all x1, blocking collectives, on_device(): lax.all_to_all(sent_rows, 'sp', split_axis=0, concat_axis=0, tiled=True)  44.2 us
    all_to_all x1, blocking collectives, on_device(): lax.all_to_all(summed, 'sp', split_axis=0, concat_axis=0, tiled=True)  42.3 us
    all_to_all x1, blocking collectives, on_device(): lax.all_to_all(sent_cots, 'sp', split_axis=0, concat_axis=0, tiled=True)  40.2 us
    all_gather x1, waiting for transfers between devices, on_device(): lax.all_gather(lax.all_to_all(sent_cots, 'sp', split_axis=0, concat_axis=...  30.3 us
    all_gather x1, waiting for transfers between devices, on_device(): lax.all_gather(own_grad.astype(bf16), 'tp', axis=1, tiled=True).astype(f32)  14.1 us
    reshape x1, local copies, waits for them, and re-layouts, on_device(): jnp.concatenate(lax.all_gather(lax.all_to_all(sent_cots, 'sp', split_axis...  10.2 us
  transfers between devices with their start and end apart: 7, of which 4 were waited for; matrix products, arithmetic and copies ran while one was open for 9% of the time, Pallas kernels for 0%

profile of v1, /device:TPU:0, one launch (start us, length us, event | category | flops | bytes accessed | tf_op | source)
XLA Modules:
  0.0 376.9 jit_solution(11734461016508358612)
XLA Ops:
  7.2 0.0 copy-start
  7.2 0.0 all-gather.5.cloned.1.call-start
  7.3 3.6 convert_element_type.75
  10.8 0.0 copy-done.2
  10.9 0.4 multiply_reduce_fusion.1
  11.3 0.1 convolution_convert_fusion.3
  11.4 0.1 select_reduce_fusion
  11.5 0.1 dynamic-slice
  11.6 2.2 convolution_convert_fusion.1
  13.8 44.2 %all_to_all.24 = bf16[8,192,512]{2,1,0:T(8,128)(2,1)} all-to-all(bf16[8,192,512]{2,1,0:T(8,128)(2,1)S(1)} %bitcast.58), channel_id=1, replica_groups=mesh['sp'=8,'tp'=4] {'sp'}, dimensions={0} | all-to-all | bytes 3145728 | tf_op jit(solution)/shard_map/all_to_all | solution.py:95
  58.0 0.0 all-gather.5.cloned.1.call-update
  58.1 0.0 all-gather.9.cloned.1.call-start
  58.1 2.0 convolution_convert_fusion
  60.1 0.0 copy-start.19
  60.1 40.2 %all_to_all.25 = bf16[8,192,512]{2,1,0:T(8,128)(2,1)} all-to-all(bf16[8,192,512]{2,1,0:T(8,128)(2,1)S(1)} %bitcast.59), channel_id=1, replica_groups=mesh['sp'=8,'tp'=4] {'sp'}, dimensions={0} | all-to-all | bytes 3145728 | tf_op jit(solution)/shard_map/all_to_all | solution.py:102
  100.3 0.0 all-gather.9.cloned.1.call-update
  100.3 0.0 reduce-scatter.3.cloned.1.call-start
  100.4 0.6 add_reduce_fusion
  101.0 0.1 all_to_all.17
  101.1 9.9 %all_to_all.26 = f32[8,1,192]{2,1,0:T(1,128)S(1)} all-to-all(f32[8,1,192]{2,1,0:T(1,128)S(1)} %all_to_all.17), channel_id=1, replica_groups=mesh['sp'=8,'tp'=4] {'sp'}, dimensions={0} | all-to-all | bytes 12288 | tf_op jit(solution)/shard_map/all_to_all | solution.py:93
  110.9 0.1 mul.171
  111.0 6.7 %fusion.17 = f32[1536,256]{1,0:T(8,128)} fusion(bf16[1536,2048]{1,0:T(8,128)(2,1)} %bitcast.66, bf16[1,2048,256]{2,1,0:T(8,128)(2,1)S(1)} %copy-done), kind=kOutput, calls=%fused_computation.32 | convolution fusion | flops 1610612736 | bytes 8912896 | tf_op jit(solution)/shard_map/dot_general | solution.py:18
  117.7 0.5 copy-done.21
  118.2 3.0 fusion.20
  121.2 30.3 %all-gather.9.cloned.1.call-done = bf16[32,192,512]{2,1,0:T(8,128)(2,1)} async-done(((bf16[8,192,512]{2,1,0:T(8,128)(2,1)}), bf16[32,192,512]{2,1,0:T(8,128)(2,1)}) %all-gather.9.cloned.1.call-update) | async-done | bytes 6291472 | tf_op jit(solution)/shard_map/all_gather | solution.py:101
  151.5 10.2 %copy.31 = bf16[8,192,4,512]{3,2,1,0:T(4,128)(2,1)} copy(bf16[8,192,4,512]{3,1,0,2:T(8,128)(2,1)} %bitcast.56) | data formatting | bytes 12582912 | tf_op jit(solution)/shard_map/reshape | solution.py:100
  161.8 5.6 %copy.32 = bf16[192,8,4,512]{3,1,2,0:T(8,128)(2,1)S(1)} copy(bf16[192,8,4,512]{3,2,1,0:T(4,128)(2,1)} %bitcast.50) | data formatting | bytes 12582912
  167.5 2.8 multiply_convert_fusion.1
  170.2 0.0 copy-start.6
  170.3 0.0 copy-start.9
  170.3 1.8 fusion.15
  172.1 4.4 %add_convert_fusion = bf16[1536,2048]{1,0:T(8,128)(2,1)} fusion(f32[1536,2048]{1,0:T(8,128)S(1)} %fusion.15, bf16[1536,256]{1,0:T(8,128)(2,1)S(1)} %get-tuple-element.16, bf16[1,2048,256]{2,1,0:T(8,128)(2,1)S(1)} %copy-done.9), kind=kOutput, calls=%fused_computation | convolution fusion | flops 1616904192 | bytes 20709376 | tf_op jit(solution)/shard_map/rf,df->rd/dot_general | solution.py:32
  176.6 0.0 reduce-scatter.3.cloned.1.call-update
  176.6 0.0 all-gather.7.cloned.1.call-start
  176.6 58.0 %reduce-scatter.3.cloned.1.call-done = bf16[8,192,512]{2,1,0:T(8,128)(2,1)} async-done(((bf16[8,192,2048]{2,1,0:T(8,128)(2,1)}), bf16[8,192,512]{2,1,0:T(8,128)(2,1)}) %reduce-scatter.3.cloned.1.call-update) | async-done | bytes 1572880 | tf_op jit(solution)/shard_map/reduce_scatter | solution.py:119
  234.6 42.3 %all_to_all.27 = bf16[8,192,512]{2,1,0:T(8,128)(2,1)S(1)} all-to-all(bf16[8,192,512]{2,1,0:T(8,128)(2,1)} %reduce-scatter.3.cloned.1.call-done), channel_id=1, replica_groups=mesh['sp'=8,'tp'=4] {'sp'}, dimensions={0} | all-to-all | bytes 3145728 | tf_op jit(solution)/shard_map/all_to_all | solution.py:123
  277.0 1.6 fusion.6
  278.5 0.0 all-gather.7.cloned.1.call-update
  278.6 0.0 reduce-scatter.5.cloned.1.call-start
  278.7 3.6 collective-permute-start
  282.4 0.0 copy-start.17
  282.4 14.1 %all-gather.7.cloned.1.call-done = bf16[384,2048]{1,0:T(8,128)(2,1)} async-done(((bf16[384,512]{1,0:T(8,128)(2,1)}), bf16[384,2048]{1,0:T(8,128)(2,1)}) %all-gather.7.cloned.1.call-update) | async-done | bytes 1572880 | tf_op jit(solution)/shard_map/all_gather | solution.py:127
  296.4 2.1 multiply_reduce_fusion
  298.6 0.0 copy-start.23
  298.6 0.0 copy-start.24
  298.6 2.5 subtract_convert_fusion
  301.1 0.0 copy-start.5
  301.1 0.0 collective-permute-done
  301.2 1.4 multiply_convert_fusion.4
  302.6 1.8 convolution_convert_fusion.2
  304.4 0.0 reduce-scatter.5.cloned.1.call-update
  304.4 0.0 slice-start.1
  304.4 0.0 copy-start.26
  304.4 0.0 copy-start.28
  304.5 6.2 %convolution_bitcast_fusion.2 = f32[1,2048,256]{2,1,0:T(8,128)} fusion(bf16[1536,2048]{1,0:T(8,128)(2,1)} %bitcast.67, bf16[1536,256]{1,0:T(8,128)(2,1)S(1)} %copy-done.7), kind=kOutput, calls=%fused_computation.10 | convolution fusion | flops 1610612736 | bytes 9175040 | tf_op jit(solution)/shard_map/rd,rf->df/dot_general | solution.py:30
  310.7 3.3 convolution_bitcast_fusion
  314.0 1.4 collective-permute-start.1
  315.4 0.0 copy-start.1
  315.4 6.1 %convolution_bitcast_fusion.1 = f32[1,2048,256]{2,1,0:T(8,128)} fusion(bf16[1536,2048]{1,0:T(8,128)(2,1)} %bitcast.68, bf16[1536,256]{1,0:T(8,128)(2,1)S(1)} %copy-done.11), kind=kOutput, calls=%fused_computation.9 | convolution fusion | flops 1610612736 | bytes 9175040 | tf_op jit(solution)/shard_map/rd,rf->df/dot_general | solution.py:31
  321.5 0.0 collective-permute-done.1
  321.5 0.8 fusion.35
  322.4 0.7 fusion.36
  323.1 45.7 %reduce-scatter.5.cloned.1.call-done = bf16[256,256]{1,0:T(8,128)(2,1)} async-done(((bf16[2048,256]{1,0:T(8,128)(2,1)}), bf16[256,256]{1,0:T(8,128)(2,1)}) %reduce-scatter.5.cloned.1.call-update) | async-done | bytes 131088 | tf_op jit(solution)/shard_map/reduce_scatter | solution.py:142
  368.8 1.6 convert_element_type.92
  (61 shorter events, 0.2 us)
Async XLA Ops:
  7.2 103.9 %copy-start = (bf16[1,2048,256]{2,1,0:T(8,128)(2,1)S(1)}, bf16[1,2048,256]{2,1,0:T(8,128)(2,1)}, u32[]{:S(2)}) copy-start(bf16[1,2048,256]{2,1,0:T(8,128)(2,1)} %param.18) | copy-start | bytes 3145732
  7.2 103.8 %all-gather.5.cloned.1.call-start = ((), (), s32[]{:S(2)}) async-start(), calls=%async_computation.6 | async-start | bytes 7864320 | tf_op jit(solution)/shard_map/all_gather | solution.py:94
  7.2 3.6 copy-start.2
  7.2 4.0 %copy-start.16 = (s32[384,2]{0,1:T(2,128)S(1)}, s32[384,2]{0,1:T(2,128)}, u32[]{:S(2)}) copy-start(s32[384,2]{0,1:T(2,128)} %param.16) | copy-start | bytes 9220
  7.3 4.3 %copy-start.15 = (f32[2048]{0:T(1024)S(1)}, f32[2048]{0:T(1024)}, u32[]{:S(2)}) copy-start(f32[2048]{0:T(1024)} %param.15) | copy-start | bytes 24580
  58.1 93.5 %all-gather.9.cloned.1.call-start = ((), (), s32[]{:S(2)}) async-start(), calls=%async_computation.10 | async-start | bytes 7864320 | tf_op jit(solution)/shard_map/all_gather | solution.py:101
  60.1 40.3 %copy-start.19 = (f32[384,2]{0,1:T(2,128)S(1)}, f32[384,2]{0,1:T(2,128)}, u32[]{:S(2)}) copy-start(f32[384,2]{0,1:T(2,128)} %param.17) | copy-start | bytes 9220
  100.3 134.3 %reduce-scatter.3.cloned.1.call-start = ((), (), s32[]{:S(2)}) async-start(), calls=%async_computation.7 | async-start | bytes 7864320 | tf_op jit(solution)/shard_map/reduce_scatter | solution.py:119
  111.0 6.7 %copy-start.8 = (bf16[1,2048,256]{2,1,0:T(8,128)(2,1)S(1)}, bf16[1,2048,256]{2,1,0:T(8,128)(2,1)}, u32[]{:S(2)}) copy-start(bf16[1,2048,256]{2,1,0:T(8,128)(2,1)} %param.19) | copy-start | bytes 3145732
  111.0 7.2 %copy-start.21 = (bf16[8,192,2048]{2,1,0:T(8,128)(2,1)S(1)}, bf16[8,192,2048]{2,1,0:T(8,128)(2,1)}, u32[]{:S(2)}) copy-start(bf16[8,192,2048]{2,1,0:T(8,128)(2,1)} %all-gather.5.cloned.1.call-done) | copy-start | bytes 18874372
  161.8 5.7 %copy-start.22 = (bf16[1,256,2048]{2,1,0:T(8,128)(2,1)S(1)}, bf16[1,256,2048]{2,1,0:T(8,128)(2,1)}, u32[]{:S(2)}) copy-start(bf16[1,256,2048]{2,1,0:T(8,128)(2,1)} %param.20) | copy-start | bytes 3145732
  161.8 5.7 %copy-start.25 = (f32[1536,256]{1,0:T(8,128)S(1)}, f32[1536,256]{1,0:T(8,128)}, u32[]{:S(2)}) copy-start(f32[1536,256]{1,0:T(8,128)} %fusion.17) | copy-start | bytes 4718596
  161.8 5.7 %copy-start.27 = (f32[1536,256]{1,0:T(8,128)S(1)}, f32[1536,256]{1,0:T(8,128)}, u32[]{:S(2)}) copy-start(f32[1536,256]{1,0:T(8,128)} %fusion.20) | copy-start | bytes 4718596
  167.4 2.8 copy-start.3
  170.2 1.9 copy-start.6
  170.2 1.9 copy-start.10
  170.3 1.9 copy-start.9
  176.6 119.8 %all-gather.7.cloned.1.call-start = ((), (), s32[]{:S(2)}) async-start(), calls=%async_computation.8 | async-start | bytes 1966080 | tf_op jit(solution)/shard_map/all_gather | solution.py:127
  277.0 1.7 copy-start.12
  277.0 1.7 copy-start.13
  277.0 5.4 %copy-start.20 = (f32[3,256]{1,0:T(4,128)S(1)}, f32[3,256]{1,0:T(4,128)}, u32[]{:S(2)}) copy-start(f32[3,256]{1,0:T(4,128)} %param.25) | copy-start | bytes 9220
  278.6 90.2 %reduce-scatter.5.cloned.1.call-start = ((), (), s32[]{:S(2)}) async-start(), calls=%async_computation.9 | async-start | bytes 1179648 | tf_op jit(solution)/shard_map/reduce_scatter | solution.py:142
  278.7 22.4 %collective-permute-start = (f32[2,256]{1,0:T(2,128)S(1)}, f32[2,256]{1,0:T(2,128)S(1)}, u32[]{:S(2)}, u32[]{:S(2)}) collective-permute-start(f32[2,256]{1,0:T(2,128)S(1)} %slice.57), channel_id=1, source_target_pairs={{0,4},{4,8},{8,12},{12,16},{16,20},{20,24},{24,28},{1,5},{5,9},{9,... | collective-permute-start | bytes 6152 | tf_op jit(solution)/shard_map/ppermute | solution.py:12
  282.4 18.8 %copy-start.17 = (f32[1,256]{1,0:T(1,128)}, f32[1,256]{1,0:T(1,128)S(1)}, u32[]{:S(2)}) copy-start(f32[1,256]{1,0:T(1,128)S(1)} %get-tuple-element.21) | copy-start | bytes 3076
  296.4 2.1 copy-start.4
  298.6 2.6 copy-start.23
  298.6 2.6 copy-start.24
  301.1 1.5 copy-start.5
  302.6 1.8 copy-start.7
  304.4 6.2 %slice-start = ((s8[6291456]{0:T(1024)(128)(4,1)}), s8[2097152]{0:T(1024)(128)(4,1)S(1)}, s32[]{:S(2)}) async-start(s8[6291456]{0:T(1024)(128)(4,1)} %bitcast.53), calls=%async_computation.11 | async-start | bytes 4194304
  304.4 6.2 %slice-start.1 = ((s8[6291456]{0:T(1024)(128)(4,1)}), s8[4194304]{0:T(1024)(128)(4,1)S(1)}, s32[]{:S(2)}) async-start(s8[6291456]{0:T(1024)(128)(4,1)} %bitcast.53), calls=%async_computation.12 | async-start | bytes 8388608
  304.4 6.2 %copy-start.26 = (f32[1536,256]{1,0:T(8,128)S(1)}, f32[1536,256]{1,0:T(8,128)}, u32[]{:S(2)}) copy-start(f32[1536,256]{1,0:T(8,128)} %fusion.17) | copy-start | bytes 4718596
  304.4 6.2 %copy-start.28 = (f32[1536,256]{1,0:T(8,128)S(1)}, f32[1536,256]{1,0:T(8,128)}, u32[]{:S(2)}) copy-start(f32[1536,256]{1,0:T(8,128)} %fusion.20) | copy-start | bytes 4718596
  310.7 3.3 copy-start.14
  310.7 4.7 %copy-start.11 = (bf16[1536,256]{1,0:T(8,128)(2,1)S(1)}, bf16[1536,256]{1,0:T(8,128)(2,1)}, u32[]{:S(2)}) copy-start(bf16[1536,256]{1,0:T(8,128)(2,1)} %copy-done.10) | copy-start | bytes 2359300
  314.0 7.6 %copy-start.18 = (f32[1,256]{1,0:T(1,128)S(1)}, f32[1,256]{1,0:T(1,128)}, u32[]{:S(2)}) copy-start(f32[1,256]{1,0:T(1,128)} %copy-done.17) | copy-start | bytes 3076
  314.0 7.6 %collective-permute-start.1 = (f32[2,256]{1,0:T(2,128)S(1)}, f32[2,256]{1,0:T(2,128)S(1)}, u32[]{:S(2)}, u32[]{:S(2)}) collective-permute-start(f32[2,256]{1,0:T(2,128)S(1)} %slice.60), channel_id=1, source_target_pairs={{4,0},{8,4},{12,8},{16,12},{20,16},{24,20},{28,24},{5,1},{9,5},{13... | collective-permute-start | bytes 6152 | tf_op jit(solution)/shard_map/ppermute | solution.py:12
  315.4 55.0 %copy-start.1 = (bf16[1,2048,256]{2,1,0:T(8,128)(2,1)S(1)}, bf16[1,2048,256]{2,1,0:T(8,128)(2,1)}, u32[]{:S(2)}) copy-start(bf16[1,2048,256]{2,1,0:T(8,128)(2,1)} %param.18) | copy-start | bytes 3145732
Sparse Core Ops, SparseCore 0:
  58.2 45.3 all-gather.4
  105.1 46.3 all-gather.8
  176.7 57.8 reduce-scatter.2
  278.7 17.7 all-gather.6
  304.5 64.1 reduce-scatter.4
